TPU v7x, 32 devices: a whole 2x2x4 slice. The times are simulated.
32 devices in a mesh: sp: 16 (over z, y, core), tp: 2 (over x).
Axes of the slice: x: 2, y: 2, z: 4, core: 2. Of those that a mesh axis runs over, the one named last changes fastest.
Arguments:
- queries: bfloat16 [3072, 1024], P('sp', 'tp'), may hold values from -6 to 6
- keys: bfloat16 [3072, 512], P('sp', 'tp'), may hold values from -6 to 6
- values: bfloat16 [3072, 512], P('sp', 'tp'), may hold values from -6 to 6
- q_gain: float32 [64], replicated, may hold values from 0.1 to 6.5
- k_gain: float32 [64], replicated, may hold values from 0.1 to 6.5
- w_out: bfloat16 [1024, 2048], P('tp'), may hold values from -12 to 12
- residual: bfloat16 [3072, 2048], P(('sp', 'tp')), may hold values from -6 to 6
- norm_gain: float32 [2048], replicated, may hold values from 0.1 to 1.9
- w_gate: bfloat16 [2048, 5632], P('sp', 'tp'), may hold values from -0.125 to 0.125
- w_up: bfloat16 [2048, 5632], P('sp', 'tp'), may hold values from -0.125 to 0.125
- w_down: bfloat16 [5632, 2048], P('tp', 'sp'), may hold values from -0.25 to 0.25
Outputs:
- layer_out: bfloat16 [3072, 2048], P(('sp', 'tp'))
All inputs are finite; a program needn't handle non-finite values.
Results may differ from a plain program's by a relative error of at most 0.018.
The roundings to bfloat16 on the way count: a program that leaves them out, or rounds other values in their place, can miss the bound.
Values may be sent and summed in bfloat16 or wider, within the bound.
A program may use at most 128 MiB of HBM per device.

v0:
```python
import math
import jax
import jax.numpy as jnp
from jax import lax
from jax.sharding import PartitionSpec as P

GRID_W = 128
EPS = 1e-06
THETA = 10000.0


def turn_half(part, angle):
    quarter = part.shape[-1] // 2
    cos_table = jnp.cos(angle)[:, None, :]
    sin_table = jnp.sin(angle)[:, None, :]
    first_part = part[..., :quarter]
    second_part = part[..., quarter:]
    return jnp.concatenate(
        [
            first_part * cos_table - second_part * sin_table,
            first_part * sin_table + second_part * cos_table,
        ],
        axis=-1,
    )


def head_norm_rope(flat, gain, offset, head_count):
    tok_rows = flat.shape[0]
    head_size = flat.shape[1] // head_count
    heads = flat.astype(jnp.float32).reshape(tok_rows, head_count, head_size)
    heads = heads * lax.rsqrt(jnp.mean(heads * heads, axis=-1, keepdims=True) + EPS) * gain
    positions = offset + jnp.arange(tok_rows, dtype=jnp.int32)
    row_pos = (positions // GRID_W).astype(jnp.float32)
    col_pos = (positions % GRID_W).astype(jnp.float32)
    half_size = head_size // 2
    inv_freq = THETA ** (-jnp.arange(0, half_size, 2, dtype=jnp.float32) / half_size)
    turned = jnp.concatenate(
        [
            turn_half(heads[..., :half_size], row_pos[:, None] * inv_freq[None, :]),
            turn_half(heads[..., half_size:], col_pos[:, None] * inv_freq[None, :]),
        ],
        axis=-1,
    )
    return turned.reshape(tok_rows, head_count * head_size).astype(jnp.bfloat16)


def body(queries, keys, values, q_gain, k_gain, w_out, residual, norm_gain, w_gate, w_up, w_down):
    tok_rows = queries.shape[0]
    head_size = q_gain.shape[0]
    q_heads = queries.shape[1] // head_size
    kv_heads = keys.shape[1] // head_size
    q_group = q_heads // kv_heads
    offset = lax.axis_index("sp") * tok_rows
    q_rot = head_norm_rope(queries, q_gain, offset, q_heads)
    k_rot = head_norm_rope(keys, k_gain, offset, kv_heads)
    query_groups = q_rot.reshape(tok_rows, kv_heads, q_group, head_size)
    score_scale = head_size ** (-0.5)
    start_state = (
        jnp.full((kv_heads, q_group, tok_rows), -1e30, jnp.float32),
        jnp.zeros((kv_heads, q_group, tok_rows), jnp.float32),
        jnp.zeros((kv_heads, q_group, tok_rows, head_size), jnp.float32),
    )
    running = start_state
    key_piece = lax.all_gather(k_rot, "sp", axis=0, tiled=True)
    value_piece = lax.all_gather(values, "sp", axis=0, tiled=True)
    piece_len = key_piece.shape[0]
    block_len = math.gcd(piece_len, 512)
    blocks = piece_len // block_len
    key_blocks = key_piece.reshape(blocks, block_len, kv_heads, head_size)
    value_blocks = value_piece.reshape(blocks, block_len, kv_heads, head_size)

    def update(state, block_pair):
        prior_max, totals, accum = state
        key_block, value_block = block_pair
        scores = (
            jnp.einsum(
                "qhgd,khd->hgqk", query_groups, key_block, preferred_element_type=jnp.float32
            )
            * score_scale
        )
        new_max = jnp.maximum(prior_max, jnp.max(scores, axis=-1))
        weights = jnp.exp(scores - new_max[..., None])
        factor = jnp.exp(prior_max - new_max)
        totals = totals * factor + jnp.sum(weights, axis=-1)
        accum = accum * factor[..., None] + jnp.einsum(
            "hgqk,khd->hgqd",
            weights.astype(jnp.bfloat16),
            value_block,
            preferred_element_type=jnp.float32,
        )
        return ((new_max, totals, accum), None)

    running, unused = lax.scan(update, running, (key_blocks, value_blocks))
    final_max, totals, accum = running
    mixed = accum / totals[..., None]
    attn = (
        jnp.transpose(mixed, (2, 0, 1, 3))
        .reshape(tok_rows, q_heads * head_size)
        .astype(jnp.bfloat16)
    )
    own_rows = lax.all_to_all(attn, "tp", split_axis=0, concat_axis=1, tiled=True)
    columns = own_rows
    proj = jnp.dot(
        columns, lax.all_gather(w_out, "tp", axis=0, tiled=True), preferred_element_type=jnp.float32
    )
    mid = residual.astype(jnp.float32) + proj
    normed = (
        mid * lax.rsqrt(jnp.mean(mid * mid, axis=-1, keepdims=True) + EPS) * norm_gain
    ).astype(jnp.bfloat16)
    gathered = lax.all_gather(normed, "tp", axis=0, tiled=True)
    columns = gathered
    gate = jnp.dot(
        columns,
        lax.all_gather(w_gate, "sp", axis=0, tiled=True),
        preferred_element_type=jnp.float32,
    )
    up_part = jnp.dot(
        columns, lax.all_gather(w_up, "sp", axis=0, tiled=True), preferred_element_type=jnp.float32
    )
    hidden = (jax.nn.silu(gate) * up_part).astype(jnp.bfloat16)
    terms = jnp.dot(
        hidden, lax.all_gather(w_down, "sp", axis=1, tiled=True), preferred_element_type=jnp.float32
    )
    down = lax.psum_scatter(
        terms.astype(jnp.bfloat16), "tp", scatter_dimension=0, tiled=True
    ).astype(jnp.float32)
    return (mid + 0.5 * down).astype(jnp.bfloat16)


def solution(mesh):
    return jax.shard_map(
        body,
        mesh=mesh,
        in_specs=(
            P("sp", "tp"),
            P("sp", "tp"),
            P("sp", "tp"),
            P(),
            P(),
            P("tp", None),
            P(("sp", "tp"), None),
            P(),
            P("sp", "tp"),
            P("sp", "tp"),
            P("tp", "sp"),
        ),
        out_specs=P(("sp", "tp"), None),
        check_vma=False,
    )
```

profile of v0, /device:TPU:0, one launch (start us, length us, event | category | flops | bytes accessed | tf_op | source)
XLA Modules:
  0.0 477.9 jit_solution(934830852998414411)
XLA Ops:
  13.3 38.7 %all-gather.7.cloned.1.call-done = bf16[3072,256]{1,0:T(8,128)(2,1)} async-done(((bf16[192,256]{1,0:T(8,128)(2,1)}), bf16[3072,256]{1,0:T(8,128)(2,1)}) %all-gather.7.cloned.1.call-update) | async-done | bytes 1572880 | tf_op jit(solution)/shard_map/all_gather | solution.py:64
  52.0 4.6 reshape.207
  56.6 3.3 copy.28
  59.9 32.7 %all-gather.9.cloned.1.call-done = bf16[3072,256]{1,0:T(8,128)(2,1)} async-done(((bf16[192,256]{1,0:T(8,128)(2,1)}), bf16[3072,256]{1,0:T(8,128)(2,1)}) %all-gather.9.cloned.1.call-update) | async-done | bytes 1572880 | tf_op jit(solution)/shard_map/all_gather | solution.py:65
  92.6 4.6 reshape.208
  97.2 3.3 copy.29
  100.5 32.2 %while.15 = (s32[]{:T(128)}, f32[4,2,192]{2,1,0:T(2,128)S(1)}, f32[4,2,192]{2,1,0:T(2,128)S(1)}, f32[4,2,192,64]{2,3,1,0:T(8,128)}, bf16[6,512,4,64]{1,3,2,0:T(8...) while((s32[]{:T(128)}, f32[4,2,192]{2,1,0:T(2,128)S(1)}, ...), condition=%wide.region_5.6_spmd.clone, body=%wide.region_2.5_spmd.clone.sunk | while | flops 207920640 | bytes 14189729 | solution.py:93
  103.4 1.8 fusion.52
  108.7 1.8 fusion.52
  114.1 1.8 fusion.52
  119.4 1.8 fusion.52
  124.8 1.8 fusion.52
  130.2 1.8 fusion.52
  134.2 10.3 %all_to_all.16 = bf16[2,96,512]{2,1,0:T(8,128)(2,1)S(1)} all-to-all(bf16[2,96,512]{2,1,0:T(8,128)(2,1)S(1)} %copy.30), channel_id=1, replica_groups=mesh['sp'=16,'tp'=2] {'tp'}, dimensions={0} | all-to-all | bytes 393216 | tf_op jit(solution)/shard_map/all_to_all | solution.py:101
  144.5 7.2 %all-gather.11.cloned.1.call-done = bf16[1024,2048]{1,0:T(8,128)(2,1)} async-done(((bf16[512,2048]{1,0:T(8,128)(2,1)}), bf16[1024,2048]{1,0:T(8,128)(2,1)}) %all-gather.11.cloned.1.call-update) | async-done | bytes 4194320 | tf_op jit(solution)/shard_map/all_gather | solution.py:104
  151.7 3.2 multiply_reduce_fusion
  155.1 11.5 %all_gather.24 = bf16[192,2048]{1,0:T(8,128)(2,1)S(1)} all-gather(bf16[96,2048]{1,0:T(8,128)(2,1)S(1)} %multiply_convert_fusion), channel_id=1, replica_groups=mesh['sp'=16,'tp'=2] {'tp'}, dimensions={0}, use_global_device_ids=true | all-gather | bytes 1179648 | tf_op jit(solution)/shard_map/all_gather | solution.py:110
  166.6 81.3 %all-gather.13.cloned.1.call-done = bf16[2048,2816]{1,0:T(8,128)(2,1)} async-done(((bf16[128,2816]{1,0:T(8,128)(2,1)}), bf16[2048,2816]{1,0:T(8,128)(2,1)}) %all-gather.13.cloned.1.call-update) | async-done | bytes 11534352 | tf_op jit(solution)/shard_map/all_gather | solution.py:114
  247.9 8.0 %fusion.30 = f32[192,2816]{1,0:T(8,128)} fusion(bf16[192,2048]{1,0:T(8,128)(2,1)S(1)} %all_gather.24, bf16[2048,2816]{1,0:T(8,128)(2,1)} %all-gather.13.cloned.1.call-done), kind=kOutput, calls=%fused_computation.69 | convolution fusion | flops 2214592512 | bytes 14483456 | tf_op jit(solution)/shard_map/dot_general | solution.py:112
  255.9 86.4 %all-gather.15.cloned.1.call-done = bf16[2048,2816]{1,0:T(8,128)(2,1)} async-done(((bf16[128,2816]{1,0:T(8,128)(2,1)}), bf16[2048,2816]{1,0:T(8,128)(2,1)}) %all-gather.15.cloned.1.call-update) | async-done | bytes 11534352 | tf_op jit(solution)/shard_map/all_gather | solution.py:118
  342.3 97.2 %all-gather.17.cloned.1.call-done = bf16[2816,2048]{1,0:T(8,128)(2,1)} async-done(((bf16[2816,128]{1,0:T(8,128)(2,1)}), bf16[2816,2048]{1,0:T(8,128)(2,1)}) %all-gather.17.cloned.1.call-update) | async-done | bytes 11534352 | tf_op jit(solution)/shard_map/all_gather | solution.py:122
  439.4 13.9 %convolution_convert_fusion = bf16[192,2048]{1,0:T(8,128)(2,1)} fusion(bf16[2816,2048]{1,0:T(8,128)(2,1)} %all-gather.17.cloned.1.call-done, bf16[192,2048]{1,0:T(8,128)(2,1)S(1)} %all_gather.24, bf16[2048,2816]{1,0:T(8,128)(2,1)} %all-gather.15.cloned.1.call-done, f32[192,2816]{1,0:T(8,128)} %fusion.30), kind=kOutput, calls=%fused_computation.25 | convolution fusion | flops 4432822272 | bytes 26804224 | tf_op jit(solution)/shard_map/dot_general | solution.py:121
  453.3 15.8 %reduce-scatter.2.cloned.1.call-done = bf16[96,2048]{1,0:T(8,128)(2,1)} async-done(((bf16[192,2048]{1,0:T(8,128)(2,1)}), bf16[96,2048]{1,0:T(8,128)(2,1)}) %reduce-scatter.2.cloned.1.call-update) | async-done | bytes 393232 | tf_op jit(solution)/shard_map/reduce_scatter | solution.py:124
  469.2 1.8 add_convert_fusion
  (99 shorter events, 29.3 us)
Async XLA Ops:
  6.5 6.3 %copy-start.2 = (bf16[192,512]{1,0:T(8,128)(2,1)S(1)}, bf16[192,512]{1,0:T(8,128)(2,1)}, u32[]{:S(2)}) copy-start(bf16[192,512]{1,0:T(8,128)(2,1)} %param.13) | copy-start | bytes 589828
  6.5 45.4 %all-gather.7.cloned.1.call-start = ((), (), s32[]{:S(2)}) async-start(), calls=%async_computation.2 | async-start | bytes 1671168 | tf_op jit(solution)/shard_map/all_gather | solution.py:64
  8.4 4.6 copy-start.4
  9.5 83.1 %all-gather.9.cloned.1.call-start = ((), (), s32[]{:S(2)}) async-start(), calls=%async_computation.3 | async-start | bytes 1671168 | tf_op jit(solution)/shard_map/all_gather | solution.py:65
  10.2 141.5 %all-gather.11.cloned.1.call-start = ((), (), s32[]{:S(2)}) async-start(), calls=%async_computation.4 | async-start | bytes 6291456 | tf_op jit(solution)/shard_map/all_gather | solution.py:104
  11.0 236.9 %all-gather.13.cloned.1.call-start = ((), (), s32[]{:S(2)}) async-start(), calls=%async_computation.5 | async-start | bytes 12255232 | tf_op jit(solution)/shard_map/all_gather | solution.py:114
  11.6 330.7 %all-gather.15.cloned.1.call-start = ((), (), s32[]{:S(2)}) async-start(), calls=%async_computation.6 | async-start | bytes 12255232 | tf_op jit(solution)/shard_map/all_gather | solution.py:118
  12.1 427.3 %all-gather.17.cloned.1.call-start = ((), (), s32[]{:S(2)}) async-start(), calls=%async_computation.7 | async-start | bytes 12255232 | tf_op jit(solution)/shard_map/all_gather | solution.py:122
  12.7 456.4 %reduce-scatter.2.cloned.1.call-start = ((), (), s32[]{:S(2)}) async-start(), calls=%async_computation.8 | async-start | bytes 1179648 | tf_op jit(solution)/shard_map/reduce_scatter | solution.py:124
  102.3 1.1 copy-start
  105.2 0.8 copy-start.1
  107.7 1.0 copy-start
  110.5 0.8 copy-start.1
  113.0 1.0 copy-start
  115.9 0.8 copy-start.1
  118.4 1.0 copy-start
  121.2 0.8 copy-start.1
  123.8 1.0 copy-start
  126.6 0.8 copy-start.1
  129.1 1.0 copy-start
  132.0 0.8 copy-start.1
  134.2 20.7 %copy-start.3 = (f32[2048]{0:T(1024)S(1)}, f32[2048]{0:T(1024)}, u32[]{:S(2)}) copy-start(f32[2048]{0:T(1024)} %param.20) | copy-start | bytes 24580
Sparse Core Ops, SparseCore 0:
  9.6 42.3 all-gather.6
  54.3 38.2 all-gather.8
  94.1 57.5 all-gather.10
  153.9 93.9 all-gather.12
  250.0 92.2 all-gather.14
  344.3 95.1 all-gather.16
  453.4 15.6 reduce-scatter.1
where the time goes:
time: 479 us; the launch traced here: 478 us
  waiting for transfers between devices  362 us (76%)
  matrix products  46 us (10%)
  local copies, waits for them, and re-layouts  23.4 us (5%)
  blocking collectives  21.8 us (5%)
  between operations  13.7 us (3%)
  other arithmetic  10.2 us (2%)
    all_gather x1, waiting for transfers between devices, body(): lax.all_gather(w_down, 'sp', axis=1, tiled=True)  97.2 us
    all_gather x1, waiting for transfers between devices, body(): lax.all_gather(w_up, 'sp', axis=0, tiled=True)  86.4 us
    all_gather x1, waiting for transfers between devices, body(): lax.all_gather(w_gate, 'sp', axis=0, tiled=True)  81.3 us
    all_gather x1, waiting for transfers between devices, body(): key_piece = lax.all_gather(k_rot, 'sp', axis=0, tiled=True)  38.7 us
    all_gather x1, waiting for transfers between devices, body(): value_piece = lax.all_gather(values, 'sp', axis=0, tiled=True)  32.7 us
    reduce_scatter x1, waiting for transfers between devices, body(): lax.psum_scatter(terms.astype(jnp.bfloat16), 'tp', scatter_dimension=0, t...  15.8 us
    dot_general x1, matrix products, body(): jnp.dot(hidden, lax.all_gather(w_down, 'sp', axis=1, tiled=True), preferr...  13.9 us
    all_gather x1, blocking collectives, body(): gathered = lax.all_gather(normed, 'tp', axis=0, tiled=True)  11.5 us
  transfers between devices with their start and end apart: 7, of which 7 were waited for; matrix products, arithmetic and copies ran while one was open for 12% of the time, Pallas kernels for 0%

commit v1 on v0

--- a/solution.py
+++ b/solution.py
@@ -61,7 +61,12 @@
         jnp.zeros((kv_heads, q_group, tok_rows, head_size), jnp.float32),
     )
     running = start_state
-    key_piece = lax.all_gather(k_rot, "sp", axis=0, tiled=True)
+    ring = [k_rot]
+    for hop in range(15):
+        ring.append(lax.ppermute(ring[-1], "sp", [(dev, (dev + 1) % 16) for dev in range(16)]))
+    key_piece = jnp.roll(
+        jnp.concatenate(ring[::-1], axis=0), (lax.axis_index("sp") + 1) * ring[0].shape[0], axis=0
+    )
     value_piece = lax.all_gather(values, "sp", axis=0, tiled=True)
     piece_len = key_piece.shape[0]
     block_len = math.gcd(piece_len, 512)

time: 479 us -> 439 us (0.916)
  waiting for transfers between devices: 362 us -> 321 us
    ppermute x0 -> x15, waiting for transfers between devices: none -> 107 us  [body(): lax.ppermute(ring[-1], 'sp', [(dev, (dev + 1) % 16) for dev in range(16)])]
    all_gather x1, waiting for transfers between devices: 81.3 us -> 11.9 us  [body(): lax.all_gather(w_gate, 'sp', axis=0, tiled=True)]
    all_gather x1 -> x0, waiting for transfers between devices: 38.7 us -> none  [body(): key_piece = lax.all_gather(k_rot, 'sp', axis=0, tiled=True)]
    all_gather x1, waiting for transfers between devices: 32.7 us -> 0.01 us  [body(): value_piece = lax.all_gather(values, 'sp', axis=0, tiled=True)]
    all_gather x1, waiting for transfers between devices: 7.22 us -> 0.02 us  [body(): lax.all_gather(w_out, 'tp', axis=0, tiled=True)]
    concatenate x0 -> x1, local copies, waits for them, and re-layouts: none -> 6.27 us  [body(): jnp.roll(jnp.concatenate(ring[::-1], axis=0), (lax.axis_index('sp') + 1)...]
  transfers between devices with their start and end apart: 7 -> 21, of which waited for: 7 -> 19; matrix products, arithmetic and copies ran while one was open for 12% -> 14% of each run, Pallas kernels for 0% -> 0%
where the time goes in v1:
time: 439 us; the launch traced here: 438 us
  waiting for transfers between devices  321 us (73%)
  matrix products  46 us (10%)
  local copies, waits for them, and re-layouts  27.8 us (6%)
  blocking collectives  17.9 us (4%)
  between operations  13.9 us (3%)
  other arithmetic  9.56 us (2%)
    ppermute x15, waiting for transfers between devices, body(): lax.ppermute(ring[-1], 'sp', [(dev, (dev + 1) % 16) for dev in range(16)])  107 us
    all_gather x1, waiting for transfers between devices, body(): lax.all_gather(w_down, 'sp', axis=1, tiled=True)  97.2 us
    all_gather x1, waiting for transfers between devices, body(): lax.all_gather(w_up, 'sp', axis=0, tiled=True)  86.4 us
    reduce_scatter x1, waiting for transfers between devices, body(): lax.psum_scatter(terms.astype(jnp.bfloat16), 'tp', scatter_dimension=0, t...  15.8 us
    dot_general x1, matrix products, body(): jnp.dot(hidden, lax.all_gather(w_down, 'sp', axis=1, tiled=True), preferr...  13.8 us
    all_gather x1, waiting for transfers between devices, body(): lax.all_gather(w_gate, 'sp', axis=0, tiled=True)  11.9 us
    dot_general x6, matrix products, update(): jnp.einsum('hgqk,khd->hgqd', weights.astype(jnp.bfloat16), value_block, p...  10.9 us
    dot_general x6, matrix products, update(): jnp.einsum('qhgd,khd->hgqk', query_groups, key_block, preferred_element_t...  10.1 us
  transfers between devices with their start and end apart: 21, of which 19 were waited for; matrix products, arithmetic and copies ran while one was open for 14% of the time, Pallas kernels for 0%

profile of v1, /device:TPU:0, one launch (start us, length us, event | category | flops | bytes accessed | tf_op | source)
XLA Modules:
  0.0 437.6 jit_solution(17263330878613538062)
XLA Ops:
  11.1 7.6 %collective-permute-done = bf16[192,256]{0,1:T(8,128)(2,1)S(1)} collective-permute-done((bf16[192,256]{0,1:T(8,128)(2,1)S(1)}, bf16[192,256]{0,1:T(8,128)(2,1)S(1)}, u32[]{:S(2)}, u32[]{:S(2)}) %collective-permute-start) | collective-permute-done | bytes 98336 | tf_op jit(solution)/shard_map/ppermute | solution.py:66
  18.8 7.3 %collective-permute-done.1 = bf16[192,256]{0,1:T(8,128)(2,1)S(1)} collective-permute-done((bf16[192,256]{0,1:T(8,128)(2,1)S(1)}, bf16[192,256]{0,1:T(8,128)(2,1)S(1)}, u32[]{:S(2)}, u32[]{:S(2)}) %collective-permute-start.1) | collective-permute-done | bytes 98336 | tf_op jit(solution)/shard_map/ppermute | solution.py:66
  26.0 7.3 %collective-permute-done.2 = bf16[192,256]{0,1:T(8,128)(2,1)S(1)} collective-permute-done((bf16[192,256]{0,1:T(8,128)(2,1)S(1)}, bf16[192,256]{0,1:T(8,128)(2,1)S(1)}, u32[]{:S(2)}, u32[]{:S(2)}) %collective-permute-start.2) | collective-permute-done | bytes 98336 | tf_op jit(solution)/shard_map/ppermute | solution.py:66
  33.4 7.1 %collective-permute-done.3 = bf16[192,256]{0,1:T(8,128)(2,1)S(1)} collective-permute-done((bf16[192,256]{0,1:T(8,128)(2,1)S(1)}, bf16[192,256]{0,1:T(8,128)(2,1)S(1)}, u32[]{:S(2)}, u32[]{:S(2)}) %collective-permute-start.3) | collective-permute-done | bytes 98336 | tf_op jit(solution)/shard_map/ppermute | solution.py:66
  40.5 7.6 %collective-permute-done.4 = bf16[192,256]{0,1:T(8,128)(2,1)S(1)} collective-permute-done((bf16[192,256]{0,1:T(8,128)(2,1)S(1)}, bf16[192,256]{0,1:T(8,128)(2,1)S(1)}, u32[]{:S(2)}, u32[]{:S(2)}) %collective-permute-start.4) | collective-permute-done | bytes 98336 | tf_op jit(solution)/shard_map/ppermute | solution.py:66
  48.2 7.1 %collective-permute-done.5 = bf16[192,256]{0,1:T(8,128)(2,1)S(1)} collective-permute-done((bf16[192,256]{0,1:T(8,128)(2,1)S(1)}, bf16[192,256]{0,1:T(8,128)(2,1)S(1)}, u32[]{:S(2)}, u32[]{:S(2)}) %collective-permute-start.5) | collective-permute-done | bytes 98336 | tf_op jit(solution)/shard_map/ppermute | solution.py:66
  55.3 7.1 %collective-permute-done.6 = bf16[192,256]{0,1:T(8,128)(2,1)S(1)} collective-permute-done((bf16[192,256]{0,1:T(8,128)(2,1)S(1)}, bf16[192,256]{0,1:T(8,128)(2,1)S(1)}, u32[]{:S(2)}, u32[]{:S(2)}) %collective-permute-start.6) | collective-permute-done | bytes 98336 | tf_op jit(solution)/shard_map/ppermute | solution.py:66
  62.3 7.1 %collective-permute-done.7 = bf16[192,256]{0,1:T(8,128)(2,1)S(1)} collective-permute-done((bf16[192,256]{0,1:T(8,128)(2,1)S(1)}, bf16[192,256]{0,1:T(8,128)(2,1)S(1)}, u32[]{:S(2)}, u32[]{:S(2)}) %collective-permute-start.7) | collective-permute-done | bytes 98336 | tf_op jit(solution)/shard_map/ppermute | solution.py:66
  69.4 7.1 %collective-permute-done.8 = bf16[192,256]{0,1:T(8,128)(2,1)S(1)} collective-permute-done((bf16[192,256]{0,1:T(8,128)(2,1)S(1)}, bf16[192,256]{0,1:T(8,128)(2,1)S(1)}, u32[]{:S(2)}, u32[]{:S(2)}) %collective-permute-start.8) | collective-permute-done | bytes 98336 | tf_op jit(solution)/shard_map/ppermute | solution.py:66
  76.8 6.9 %collective-permute-done.9 = bf16[192,256]{0,1:T(8,128)(2,1)S(1)} collective-permute-done((bf16[192,256]{0,1:T(8,128)(2,1)S(1)}, bf16[192,256]{0,1:T(8,128)(2,1)S(1)}, u32[]{:S(2)}, u32[]{:S(2)}) %collective-permute-start.9) | collective-permute-done | bytes 98336 | tf_op jit(solution)/shard_map/ppermute | solution.py:66
  83.8 7.0 %collective-permute-done.10 = bf16[192,256]{0,1:T(8,128)(2,1)S(1)} collective-permute-done((bf16[192,256]{0,1:T(8,128)(2,1)S(1)}, bf16[192,256]{0,1:T(8,128)(2,1)S(1)}, u32[]{:S(2)}, u32[]{:S(2)}) %collective-permute-start.10) | collective-permute-done | bytes 98336 | tf_op jit(solution)/shard_map/ppermute | solution.py:66
  90.8 7.1 %collective-permute-done.11 = bf16[192,256]{0,1:T(8,128)(2,1)S(1)} collective-permute-done((bf16[192,256]{0,1:T(8,128)(2,1)S(1)}, bf16[192,256]{0,1:T(8,128)(2,1)S(1)}, u32[]{:S(2)}, u32[]{:S(2)}) %collective-permute-start.11) | collective-permute-done | bytes 98336 | tf_op jit(solution)/shard_map/ppermute | solution.py:66
  98.0 7.0 %collective-permute-done.12 = bf16[192,256]{0,1:T(8,128)(2,1)S(1)} collective-permute-done((bf16[192,256]{0,1:T(8,128)(2,1)S(1)}, bf16[192,256]{0,1:T(8,128)(2,1)S(1)}, u32[]{:S(2)}, u32[]{:S(2)}) %collective-permute-start.12) | collective-permute-done | bytes 98336 | tf_op jit(solution)/shard_map/ppermute | solution.py:66
  105.2 6.9 %collective-permute-done.13 = bf16[192,256]{0,1:T(8,128)(2,1)S(1)} collective-permute-done((bf16[192,256]{0,1:T(8,128)(2,1)S(1)}, bf16[192,256]{0,1:T(8,128)(2,1)S(1)}, u32[]{:S(2)}, u32[]{:S(2)}) %collective-permute-start.13) | collective-permute-done | bytes 98336 | tf_op jit(solution)/shard_map/ppermute | solution.py:66
  112.8 6.5 %collective-permute-done.14 = bf16[192,256]{0,1:T(8,128)(2,1)} collective-permute-done((bf16[192,256]{0,1:T(8,128)(2,1)S(1)}, bf16[192,256]{0,1:T(8,128)(2,1)}, u32[]{:S(2)}, u32[]{:S(2)}) %collective-permute-start.14) | collective-permute-done | bytes 98336 | tf_op jit(solution)/shard_map/ppermute | solution.py:66
  140.5 32.4 %while.15 = (s32[]{:T(128)}, f32[4,2,192]{2,1,0:T(2,128)S(1)}, f32[4,2,192]{2,1,0:T(2,128)S(1)}, f32[4,2,192,64]{2,3,1,0:T(8,128)}, bf16[6,512,4,64]{1,3,2,0:T(8...) while((s32[]{:T(128)}, f32[4,2,192]{2,1,0:T(2,128)S(1)}, ...), condition=%wide.region_5.6_spmd.clone, body=%wide.region_2.5_spmd.clone.sunk | while | flops 207920640 | bytes 14189729 | solution.py:98
  174.3 9.3 %all_to_all.16 = bf16[2,96,512]{2,1,0:T(8,128)(2,1)S(1)} all-to-all(bf16[2,96,512]{2,1,0:T(8,128)(2,1)S(1)} %copy.28), channel_id=1, replica_groups=mesh['sp'=16,'tp'=2] {'tp'}, dimensions={0} | all-to-all | bytes 393216 | tf_op jit(solution)/shard_map/all_to_all | solution.py:106
  187.0 8.6 %all_gather.20 = bf16[192,2048]{1,0:T(8,128)(2,1)S(1)} all-gather(bf16[96,2048]{1,0:T(8,128)(2,1)S(1)} %multiply_convert_fusion), channel_id=1, replica_groups=mesh['sp'=16,'tp'=2] {'tp'}, dimensions={0}, use_global_device_ids=true | all-gather | bytes 1179648 | tf_op jit(solution)/shard_map/all_gather | solution.py:115
  195.7 11.9 %all-gather.10.cloned.1.call-done = bf16[2048,2816]{1,0:T(8,128)(2,1)} async-done(((bf16[128,2816]{1,0:T(8,128)(2,1)}), bf16[2048,2816]{1,0:T(8,128)(2,1)}) %all-gather.10.cloned.1.call-update) | async-done | bytes 11534352 | tf_op jit(solution)/shard_map/all_gather | solution.py:119
  207.6 8.0 %fusion.30 = f32[192,2816]{1,0:T(8,128)} fusion(bf16[192,2048]{1,0:T(8,128)(2,1)S(1)} %all_gather.20, bf16[2048,2816]{1,0:T(8,128)(2,1)} %all-gather.10.cloned.1.call-done), kind=kOutput, calls=%fused_computation.70 | convolution fusion | flops 2214592512 | bytes 14483456 | tf_op jit(solution)/shard_map/dot_general | solution.py:117
  215.6 86.4 %all-gather.12.cloned.1.call-done = bf16[2048,2816]{1,0:T(8,128)(2,1)} async-done(((bf16[128,2816]{1,0:T(8,128)(2,1)}), bf16[2048,2816]{1,0:T(8,128)(2,1)}) %all-gather.12.cloned.1.call-update) | async-done | bytes 11534352 | tf_op jit(solution)/shard_map/all_gather | solution.py:123
  302.0 97.2 %all-gather.14.cloned.1.call-done = bf16[2816,2048]{1,0:T(8,128)(2,1)} async-done(((bf16[2816,128]{1,0:T(8,128)(2,1)}), bf16[2816,2048]{1,0:T(8,128)(2,1)}) %all-gather.14.cloned.1.call-update) | async-done | bytes 11534352 | tf_op jit(solution)/shard_map/all_gather | solution.py:127
  399.2 13.8 %convolution_convert_fusion = bf16[192,2048]{1,0:T(8,128)(2,1)} fusion(bf16[2816,2048]{1,0:T(8,128)(2,1)} %all-gather.14.cloned.1.call-done, bf16[192,2048]{1,0:T(8,128)(2,1)S(1)} %all_gather.20, bf16[2048,2816]{1,0:T(8,128)(2,1)} %all-gather.12.cloned.1.call-done, f32[192,2816]{1,0:T(8,128)} %fusion.30), kind=kOutput, calls=%fused_computation.25 | convolution fusion | flops 4432822272 | bytes 26804224 | tf_op jit(solution)/shard_map/dot_general | solution.py:126
  413.0 15.8 %reduce-scatter.2.cloned.1.call-done = bf16[96,2048]{1,0:T(8,128)(2,1)} async-done(((bf16[192,2048]{1,0:T(8,128)(2,1)}), bf16[96,2048]{1,0:T(8,128)(2,1)}) %reduce-scatter.2.cloned.1.call-update) | async-done | bytes 393232 | tf_op jit(solution)/shard_map/reduce_scatter | solution.py:129
  (159 shorter events, 65.5 us)
Async XLA Ops:
  6.5 70.1 %copy-start.16 = (bf16[192,512]{1,0:T(8,128)(2,1)S(1)}, bf16[192,512]{1,0:T(8,128)(2,1)}, u32[]{:S(2)}) copy-start(bf16[192,512]{1,0:T(8,128)(2,1)} %param.13) | copy-start | bytes 589828
  6.5 126.0 %all-gather.6.cloned.1.call-start = ((), (), s32[]{:S(2)}) async-start(), calls=%async_computation.2 | async-start | bytes 1671168 | tf_op jit(solution)/shard_map/all_gather | solution.py:70
  7.3 90.7 %copy-start.20 = (f32[64]{0:T(128)S(1)}, f32[64]{0:T(128)}, u32[]{:S(2)}) copy-start(f32[64]{0:T(128)} %param.16) | copy-start | bytes 772
  7.3 176.4 %all-gather.8.cloned.1.call-start = ((), (), s32[]{:S(2)}) async-start(), calls=%async_computation.3 | async-start | bytes 6291456 | tf_op jit(solution)/shard_map/all_gather | solution.py:109
  8.0 199.6 %all-gather.10.cloned.1.call-start = ((), (), s32[]{:S(2)}) async-start(), calls=%async_computation.4 | async-start | bytes 12255232 | tf_op jit(solution)/shard_map/all_gather | solution.py:119
  8.8 293.2 %all-gather.12.cloned.1.call-start = ((), (), s32[]{:S(2)}) async-start(), calls=%async_computation.5 | async-start | bytes 12255232 | tf_op jit(solution)/shard_map/all_gather | solution.py:123
  9.3 389.8 %all-gather.14.cloned.1.call-start = ((), (), s32[]{:S(2)}) async-start(), calls=%async_computation.6 | async-start | bytes 12255232 | tf_op jit(solution)/shard_map/all_gather | solution.py:127
  9.9 418.9 %reduce-scatter.2.cloned.1.call-start = ((), (), s32[]{:S(2)}) async-start(), calls=%async_computation.7 | async-start | bytes 1179648 | tf_op jit(solution)/shard_map/reduce_scatter | solution.py:129
  10.6 8.2 %collective-permute-start = (bf16[192,256]{0,1:T(8,128)(2,1)S(1)}, bf16[192,256]{0,1:T(8,128)(2,1)S(1)}, u32[]{:S(2)}, u32[]{:S(2)}) collective-permute-start(bf16[192,256]{0,1:T(8,128)(2,1)S(1)} %bitcast.68), channel_id=1, source_target_pairs={{0,2},{2,4},{4,6},{6,8},{8,10},{10,12},{12,14},{14,16},{16,18},{18... | collective-permute-start | bytes 294920 | tf_op jit(solution)/shard_map/ppermute | solution.py:66
  18.7 57.8 %copy-start.2 = (bf16[192,256]{0,1:T(8,128)(2,1)}, bf16[192,256]{0,1:T(8,128)(2,1)S(1)}, u32[]{:S(2)}) copy-start(bf16[192,256]{0,1:T(8,128)(2,1)S(1)} %collective-permute-done) | copy-start | bytes 294916
  18.7 7.3 %collective-permute-start.1 = (bf16[192,256]{0,1:T(8,128)(2,1)S(1)}, bf16[192,256]{0,1:T(8,128)(2,1)S(1)}, u32[]{:S(2)}, u32[]{:S(2)}) collective-permute-start(bf16[192,256]{0,1:T(8,128)(2,1)S(1)} %collective-permute-done), channel_id=1, source_target_pairs={{0,2},{2,4},{4,6},{6,8},{8,10},{10,12},{12,14},{14,16},{16,18},{18... | collective-permute-start | bytes 294920 | tf_op jit(solution)/shard_map/ppermute | solution.py:66
  26.0 7.3 %collective-permute-start.2 = (bf16[192,256]{0,1:T(8,128)(2,1)S(1)}, bf16[192,256]{0,1:T(8,128)(2,1)S(1)}, u32[]{:S(2)}, u32[]{:S(2)}) collective-permute-start(bf16[192,256]{0,1:T(8,128)(2,1)S(1)} %collective-permute-done.1), channel_id=1, source_target_pairs={{0,2},{2,4},{4,6},{6,8},{8,10},{10,12},{12,14},{14,16},{16,18},{18... | collective-permute-start | bytes 294920 | tf_op jit(solution)/shard_map/ppermute | solution.py:66
  33.4 7.1 %collective-permute-start.3 = (bf16[192,256]{0,1:T(8,128)(2,1)S(1)}, bf16[192,256]{0,1:T(8,128)(2,1)S(1)}, u32[]{:S(2)}, u32[]{:S(2)}) collective-permute-start(bf16[192,256]{0,1:T(8,128)(2,1)S(1)} %collective-permute-done.2), channel_id=1, source_target_pairs={{0,2},{2,4},{4,6},{6,8},{8,10},{10,12},{12,14},{14,16},{16,18},{18... | collective-permute-start | bytes 294920 | tf_op jit(solution)/shard_map/ppermute | solution.py:66
  40.5 7.7 %collective-permute-start.4 = (bf16[192,256]{0,1:T(8,128)(2,1)S(1)}, bf16[192,256]{0,1:T(8,128)(2,1)S(1)}, u32[]{:S(2)}, u32[]{:S(2)}) collective-permute-start(bf16[192,256]{0,1:T(8,128)(2,1)S(1)} %collective-permute-done.3), channel_id=1, source_target_pairs={{0,2},{2,4},{4,6},{6,8},{8,10},{10,12},{12,14},{14,16},{16,18},{18... | collective-permute-start | bytes 294920 | tf_op jit(solution)/shard_map/ppermute | solution.py:66
  48.2 7.1 %collective-permute-start.5 = (bf16[192,256]{0,1:T(8,128)(2,1)S(1)}, bf16[192,256]{0,1:T(8,128)(2,1)S(1)}, u32[]{:S(2)}, u32[]{:S(2)}) collective-permute-start(bf16[192,256]{0,1:T(8,128)(2,1)S(1)} %collective-permute-done.4), channel_id=1, source_target_pairs={{0,2},{2,4},{4,6},{6,8},{8,10},{10,12},{12,14},{14,16},{16,18},{18... | collective-permute-start | bytes 294920 | tf_op jit(solution)/shard_map/ppermute | solution.py:66
  55.2 7.1 %collective-permute-start.6 = (bf16[192,256]{0,1:T(8,128)(2,1)S(1)}, bf16[192,256]{0,1:T(8,128)(2,1)S(1)}, u32[]{:S(2)}, u32[]{:S(2)}) collective-permute-start(bf16[192,256]{0,1:T(8,128)(2,1)S(1)} %collective-permute-done.5), channel_id=1, source_target_pairs={{0,2},{2,4},{4,6},{6,8},{8,10},{10,12},{12,14},{14,16},{16,18},{18... | collective-permute-start | bytes 294920 | tf_op jit(solution)/shard_map/ppermute | solution.py:66
  62.3 7.1 %collective-permute-start.7 = (bf16[192,256]{0,1:T(8,128)(2,1)S(1)}, bf16[192,256]{0,1:T(8,128)(2,1)S(1)}, u32[]{:S(2)}, u32[]{:S(2)}) collective-permute-start(bf16[192,256]{0,1:T(8,128)(2,1)S(1)} %collective-permute-done.6), channel_id=1, source_target_pairs={{0,2},{2,4},{4,6},{6,8},{8,10},{10,12},{12,14},{14,16},{16,18},{18... | collective-permute-start | bytes 294920 | tf_op jit(solution)/shard_map/ppermute | solution.py:66
  69.4 7.1 %collective-permute-start.8 = (bf16[192,256]{0,1:T(8,128)(2,1)S(1)}, bf16[192,256]{0,1:T(8,128)(2,1)S(1)}, u32[]{:S(2)}, u32[]{:S(2)}) collective-permute-start(bf16[192,256]{0,1:T(8,128)(2,1)S(1)} %collective-permute-done.7), channel_id=1, source_target_pairs={{0,2},{2,4},{4,6},{6,8},{8,10},{10,12},{12,14},{14,16},{16,18},{18... | collective-permute-start | bytes 294920 | tf_op jit(solution)/shard_map/ppermute | solution.py:66
  76.6 7.1 %collective-permute-start.9 = (bf16[192,256]{0,1:T(8,128)(2,1)S(1)}, bf16[192,256]{0,1:T(8,128)(2,1)S(1)}, u32[]{:S(2)}, u32[]{:S(2)}) collective-permute-start(bf16[192,256]{0,1:T(8,128)(2,1)S(1)} %collective-permute-done.8), channel_id=1, source_target_pairs={{0,2},{2,4},{4,6},{6,8},{8,10},{10,12},{12,14},{14,16},{16,18},{18... | collective-permute-start | bytes 294920 | tf_op jit(solution)/shard_map/ppermute | solution.py:66
  83.7 7.1 %collective-permute-start.10 = (bf16[192,256]{0,1:T(8,128)(2,1)S(1)}, bf16[192,256]{0,1:T(8,128)(2,1)S(1)}, u32[]{:S(2)}, u32[]{:S(2)}) collective-permute-start(bf16[192,256]{0,1:T(8,128)(2,1)S(1)} %collective-permute-done.9), channel_id=1, source_target_pairs={{0,2},{2,4},{4,6},{6,8},{8,10},{10,12},{12,14},{14,16},{16,18},{18... | collective-permute-start | bytes 294920 | tf_op jit(solution)/shard_map/ppermute | solution.py:66
  90.8 7.1 %collective-permute-start.11 = (bf16[192,256]{0,1:T(8,128)(2,1)S(1)}, bf16[192,256]{0,1:T(8,128)(2,1)S(1)}, u32[]{:S(2)}, u32[]{:S(2)}) collective-permute-start(bf16[192,256]{0,1:T(8,128)(2,1)S(1)} %collective-permute-done.10), channel_id=1, source_target_pairs={{0,2},{2,4},{4,6},{6,8},{8,10},{10,12},{12,14},{14,16},{16,18},{18... | collective-permute-start | bytes 294920 | tf_op jit(solution)/shard_map/ppermute | solution.py:66
  97.9 7.1 %collective-permute-start.12 = (bf16[192,256]{0,1:T(8,128)(2,1)S(1)}, bf16[192,256]{0,1:T(8,128)(2,1)S(1)}, u32[]{:S(2)}, u32[]{:S(2)}) collective-permute-start(bf16[192,256]{0,1:T(8,128)(2,1)S(1)} %collective-permute-done.11), channel_id=1, source_target_pairs={{0,2},{2,4},{4,6},{6,8},{8,10},{10,12},{12,14},{14,16},{16,18},{18... | collective-permute-start | bytes 294920 | tf_op jit(solution)/shard_map/ppermute | solution.py:66
  105.0 7.1 %collective-permute-start.13 = (bf16[192,256]{0,1:T(8,128)(2,1)S(1)}, bf16[192,256]{0,1:T(8,128)(2,1)S(1)}, u32[]{:S(2)}, u32[]{:S(2)}) collective-permute-start(bf16[192,256]{0,1:T(8,128)(2,1)S(1)} %collective-permute-done.12), channel_id=1, source_target_pairs={{0,2},{2,4},{4,6},{6,8},{8,10},{10,12},{12,14},{14,16},{16,18},{18... | collective-permute-start | bytes 294920 | tf_op jit(solution)/shard_map/ppermute | solution.py:66
  112.1 7.2 %collective-permute-start.14 = (bf16[192,256]{0,1:T(8,128)(2,1)S(1)}, bf16[192,256]{0,1:T(8,128)(2,1)}, u32[]{:S(2)}, u32[]{:S(2)}) collective-permute-start(bf16[192,256]{0,1:T(8,128)(2,1)S(1)} %collective-permute-done.13), channel_id=1, source_target_pairs={{0,2},{2,4},{4,6},{6,8},{8,10},{10,12},{12,14},{14,16},{16,18},{18... | collective-permute-start | bytes 294920 | tf_op jit(solution)/shard_map/ppermute | solution.py:66
  (28 other events, 339.4 us)
Sparse Core Ops, SparseCore 0:
  9.6 43.8 all-gather.5
  55.1 56.1 all-gather.7
  113.5 94.0 all-gather.9
  209.7 92.2 all-gather.11
  304.0 95.1 all-gather.13
  413.1 15.6 reduce-scatter.1
